TPU v7x, 512 devices: a whole 4x4x16 slice. The times are simulated.
512 devices in a mesh: sp: 128 (over z, x, core), tp: 4 (over y).
Axes of the slice: x: 4, y: 4, z: 16, core: 2. Of those that a mesh axis runs over, the one named last changes fastest.
Arguments:
- query_main: bfloat16 [16384, 2048], P('sp', 'tp'), may hold values from -6 to 6
- query_rotary: bfloat16 [16384, 1024], P('sp', 'tp'), may hold values from -7 to 7
- latent: bfloat16 [16384, 512], P('sp'), may hold values from -24 to 24
- key_rotary: bfloat16 [16384, 64], P('sp'), may hold values from -8 to 8
- key_weight: bfloat16 [512, 2048], P(None, 'tp'), may hold values from -0.25 to 0.25
- value_weight: bfloat16 [512, 2048], P(None, 'tp'), may hold values from -0.25 to 0.25
- head_output: bfloat16 [16384, 2048], P('sp', 'tp'), may hold values from -2 to 2
- output_grad: bfloat16 [16384, 2048], P('sp', 'tp'), may hold values from -128 to 128
- row_logsum: float32 [16, 16384], P('tp', 'sp'), may hold values from 3 to 16, as said below
Outputs:
- grad_query_main: float32 [16384, 2048], P('sp', 'tp')
- grad_query_rotary: float32 [16384, 1024], P('sp', 'tp')
- grad_latent: float32 [16384, 512], P('sp')
- grad_key_rotary: float32 [16384, 64], P('sp')
- grad_key_weight: float32 [512, 2048], P('sp', 'tp')
Inputs may be any that keep to these rules, and one draw needn't show every extreme that they name: With p the place of token i in its sequence and q = i % 128, row_logsum[h, i] minus the logarithm of (p + 1 + 54 (q + 1)) lies between -0.3 and 1.5.
All inputs are finite; a program needn't handle non-finite values.
Results may differ from a plain program's by a relative error of at most 0.003.
The roundings to bfloat16 on the way count: a program that leaves them out, or rounds other values in their place, can miss the bound.
Values may be sent and summed in bfloat16 or wider, within the bound.
A program may use at most 64 MiB of HBM per device.

v0:
```python
import functools
import math

import jax
import jax.numpy as jnp
from jax import lax
from jax.experimental import pallas as pl
from jax.experimental.pallas import tpu as pltpu
from jax.sharding import PartitionSpec as P

SEQ_DEVICES = 32
VMEM_BYTES = 67043328
MESH = pl.DeviceIdType.MESH
F32 = jnp.float32
BF16 = jnp.bfloat16


def dot(a, b, ca, cb, precision=None):
    return lax.dot_general(
        a, b, (((ca,), (cb,)), ((), ())), preferred_element_type=F32, precision=precision
    )


def kernel(
    dims,
    qm_h, qr_h, lat_h, rot_h, kw_h, vw_h, ho_h, og_h, logs_h,
    o_main, o_rot, o_lat, o_krot, o_kw,
    qm, qr, lat, rot, kw, vw, ho, og, logs, insem,
    lat_buf, rot_buf, ql, gr, qrp, mixed, rsum, gpart, obuf, kwst, kwrecv, fin_s, fin_r,
    ksend, krecv, fsend, frecv, finsend, finrecv, agsend, agrecv, kwsend, kwrecvs,
    *halving,
):
    n_sp, n_tp, heads, factor = dims
    stages = n_tp.bit_length() - 1
    half_s, half_r = halving[:stages], halving[stages : 2 * stages]
    half_ss, half_rs = halving[2 * stages : 3 * stages], halving[3 * stages :]
    span = min(SEQ_DEVICES, n_sp)
    lead = span // 4
    tok, width = lat.shape
    rdim = rot.shape[0]
    kdim = kw.shape[1] // heads
    vdim = vw.shape[1] // heads
    loads = [
        pltpu.make_async_copy(src, dst, insem.at[n])
        for n, (src, dst) in enumerate(
            (
                (lat_h, lat), (rot_h, rot), (qm_h, qm), (kw_h, kw), (og_h, og), (vw_h, vw),
                (ho_h, ho), (qr_h, qr), (logs_h, logs),
            )
        )
    ]
    for c in loads:
        c.start()
    sp = lax.axis_index("sp")
    tp = lax.axis_index("tp")
    seq = (sp + lead) // span
    first = jnp.maximum(seq * span - lead, 0)
    last = jnp.minimum((seq + 1) * span - lead, n_sp)
    before = sp - first
    after = last - 1 - sp
    low = tp % 2
    pair = tp + 1 - 2 * low

    barrier = pltpu.get_barrier_semaphore()

    @pl.loop(1, n_sp)
    def _(d):
        pl.semaphore_signal(
            barrier, inc=1, device_id={"sp": (sp + d) % n_sp}, device_id_type=MESH
        )

    for t in range(1, n_tp):
        pl.semaphore_signal(
            barrier, inc=1, device_id={"tp": (tp + t) % n_tp}, device_id_type=MESH
        )
    pl.semaphore_wait(barrier, n_sp - 1 + n_tp - 1)

    def part_of(side, size):
        return pl.ds(pl.multiple_of(side * (size // 2), size // 2), size // 2)

    keys = ((lat, lat_buf, tok), (rot, rot_buf, rdim))

    def key_copies(i):
        return [
            pltpu.make_async_remote_copy(
                src_ref=src.at[part_of(low, size)], dst_ref=dst.at[i, part_of(low, size)],
                send_sem=ksend.at[i, n], recv_sem=krecv.at[i, n],
                device_id={"sp": sp + i}, device_id_type=MESH,
            )
            for n, (src, dst, size) in enumerate(keys)
        ]

    def forward_copies(i, side):
        return [
            pltpu.make_async_remote_copy(
                src_ref=buf.at[i, part_of(side, size)], dst_ref=buf.at[i, part_of(side, size)],
                send_sem=fsend.at[i, n], recv_sem=frecv.at[i, n],
                device_id={"tp": pair}, device_id_type=MESH,
            )
            for n, (_, buf, size) in enumerate(keys)
        ]

    loads[0].wait()
    loads[1].wait()

    @pl.loop(1, after + 1)
    def _(i):
        for c in key_copies(i):
            c.start()

    lat_buf[0] = lat[...]
    rot_buf[0] = rot[...]
    for c in loads[2:]:
        c.wait()
    terms_parts = []
    for h in range(heads):
        rows = slice(h * tok, (h + 1) * tok)
        kcols = slice(h * kdim, (h + 1) * kdim)
        vcols = slice(h * vdim, (h + 1) * vdim)
        ql[rows] = dot(qm[:, kcols], kw[:, kcols], 1, 1).astype(BF16)
        gr[rows] = dot(og[:, vcols], vw[:, vcols], 1, 1).astype(BF16)
        qrp[rows] = jnp.concatenate(
            [qr[:, h * rdim : (h + 1) * rdim], jnp.zeros((tok, qrp.shape[1] - rdim), BF16)], axis=1
        )
        prod = ho[:, vcols].astype(F32) * og[:, vcols].astype(F32)
        terms_parts.append(
            dot(jnp.ones((8, vdim), F32), prod, 1, 1, lax.Precision.HIGHEST)[0:1]
        )
    terms = jnp.concatenate(terms_parts, axis=1)
    row_logs = jnp.concatenate([logs[h : h + 1, :] for h in range(heads)], axis=1)
    mixed[...] = jnp.zeros_like(mixed)
    rsum[...] = jnp.zeros_like(rsum)

    def level_offset(level):
        off = 0
        for b in range(level):
            off = off + ((tp // (1 << b)) % 2) * (tok >> (b + 1))
        return off

    def half_copy(s, i):
        bit = (tp // (1 << s)) % 2
        return pltpu.make_async_remote_copy(
            src_ref=half_s[s].at[i], dst_ref=half_r[s].at[i],
            send_sem=half_ss[s].at[i], recv_sem=half_rs[s].at[i],
            device_id={"tp": tp + (1 - 2 * bit) * (1 << s)}, device_id_type=MESH,
        )

    def send_half(s, i):
        size = tok >> (s + 1)
        bit = (tp // (1 << s)) % 2
        start = pl.multiple_of(level_offset(s) + (1 - bit) * size, size)
        half_s[s][i] = gpart[i, pl.ds(start, size), :].astype(BF16)
        half_copy(s, i).start()

    def fin_copy(i):
        return pltpu.make_async_remote_copy(
            src_ref=fin_s.at[i], dst_ref=fin_r.at[i],
            send_sem=finsend.at[i], recv_sem=finrecv.at[i],
            device_id={"sp": sp - i}, device_id_type=MESH,
        )

    def arrive(i):
        for c in key_copies(i):
            c.wait_recv()
        for c in forward_copies(i, low):
            c.start()

    quarter = tok >> stages
    my_rows = pl.ds(pl.multiple_of(level_offset(stages), quarter), quarter)

    def attend(i):
        @pl.when(i < before)
        def _():
            arrive(i + 1)

        @pl.when(i > 0)
        def _():
            for c in forward_copies(i, 1 - low):
                c.wait_recv()

        lt = lat_buf[i]
        rt = rot_buf[i]
        scores = dot(lt, ql[...], 1, 1) + dot(rt, qrp[:, :rdim], 0, 1)
        weights = jnp.exp(factor * scores - row_logs)
        key_at = lax.broadcasted_iota(jnp.int32, weights.shape, 0)
        query_at = lax.broadcasted_iota(jnp.int32, weights.shape, 1) % tok
        weights = jnp.where((key_at <= query_at) | (i > 0), weights, 0.0)
        slopes = dot(lt, gr[...], 1, 1)
        dscores = weights * (slopes - terms)
        wl = weights.astype(BF16)
        dl = dscores.astype(BF16)
        gpart[i, :, :width] = factor * dot(dl, ql[...], 1, 0) + dot(wl, gr[...], 1, 0)
        gpart[i, :, width:] = factor * dot(dl, qrp[...], 1, 0)
        send_half(0, i)
        mixed[...] += dot(dl, lt, 0, 0)
        rsum[...] += dot(dl, rt, 0, 1)

    @pl.loop(0, before + 1 + stages)
    def _(it):
        @pl.when(it <= before)
        def _():
            attend(it)

        for s in range(1, stages + 1):
            i = it - s

            @pl.when((i >= 0) & (i <= before))
            def _():
                half_copy(s - 1, i).wait_recv()
                size = tok >> s
                rows = pl.ds(pl.multiple_of(level_offset(s), size), size)
                gpart[i, rows, :] += half_r[s - 1][i].astype(F32)
                if s < stages:
                    send_half(s, i)
                else:

                    @pl.when(i > 0)
                    def _():
                        fin_s[i] = gpart[i, rows, :].astype(BF16)
                        fin_copy(i).start()

    part = o_kw.shape[0]

    def kw_copy(d):
        dest = (sp + d) % n_sp
        return pltpu.make_async_remote_copy(
            src_ref=kwst.at[dest], dst_ref=kwrecv.at[n_sp - d],
            send_sem=kwsend.at[d], recv_sem=kwrecvs.at[n_sp - d],
            device_id={"sp": dest}, device_id_type=MESH,
        )

    def kw_landing(d):
        return pltpu.make_async_remote_copy(
            src_ref=kwst.at[0], dst_ref=kwrecv.at[d],
            send_sem=kwsend.at[d], recv_sem=kwrecvs.at[d],
            device_id={"sp": (sp + d) % n_sp}, device_id_type=MESH,
        )

    low_parts = []
    for h in range(heads):
        rows = slice(h * tok, (h + 1) * tok)
        kcols = slice(h * kdim, (h + 1) * kdim)
        ml = mixed[rows].astype(BF16)
        term = (factor * dot(ml, qm[:, kcols], 0, 0)).astype(BF16)
        for d in range(n_sp):
            kwst[d, :, kcols] = term[d * part : (d + 1) * part]
        low_parts.append(ml)

    @pl.loop(1, n_sp)
    def _(d):
        kw_copy(d).start()

    for h in range(heads):
        rows = slice(h * tok, (h + 1) * tok)
        kcols = slice(h * kdim, (h + 1) * kdim)
        o_main[:, kcols] = factor * dot(low_parts[h], kw[:, kcols], 1, 0)
        o_rot[:, h * rdim : (h + 1) * rdim] = factor * rsum[rows]

    @pl.loop(1, after + 1)
    def _(i):
        pltpu.make_async_remote_copy(
            src_ref=fin_s.at[i], dst_ref=fin_r.at[i],
            send_sem=finsend.at[i], recv_sem=finrecv.at[i],
            device_id={"sp": sp + i}, device_id_type=MESH,
        ).wait_recv()
        gpart[0, my_rows, :] += fin_r[i].astype(F32)

    obuf[my_rows] = gpart[0, my_rows, :]

    def ag_copy(t):
        return pltpu.make_async_remote_copy(
            src_ref=obuf.at[my_rows], dst_ref=obuf.at[my_rows],
            send_sem=agsend.at[t], recv_sem=agrecv.at[n_tp - t],
            device_id={"tp": (tp + t) % n_tp}, device_id_type=MESH,
        )

    for t in range(1, n_tp):
        ag_copy(t).start()

    total = kwst[sp].astype(F32)
    for d in range(1, n_sp):
        kw_landing(d).wait_recv()
        total = total + kwrecv[d].astype(F32)
    o_kw[...] = total

    for t in range(1, n_tp):
        peer = (tp + t) % n_tp
        off = 0
        for b in range(stages):
            off = off + ((peer // (1 << b)) % 2) * (tok >> (b + 1))
        rows = pl.ds(pl.multiple_of(off, quarter), quarter)
        pltpu.make_async_remote_copy(
            src_ref=obuf.at[rows], dst_ref=obuf.at[rows],
            send_sem=agsend.at[t], recv_sem=agrecv.at[t],
            device_id={"tp": peer}, device_id_type=MESH,
        ).wait_recv()
    o_lat[...] = obuf[:, :width]
    o_krot[...] = obuf[:, width:].T[:rdim]

    @pl.loop(1, after + 1)
    def _(i):
        for c in key_copies(i):
            c.wait_send()

    @pl.loop(0, before + 1)
    def _(i):
        for s in range(stages):
            half_copy(s, i).wait_send()

        @pl.when(i > 0)
        def _():
            for c in forward_copies(i, low):
                c.wait_send()
            fin_copy(i).wait_send()

    @pl.loop(1, n_sp)
    def _(d):
        kw_copy(d).wait_send()

    for t in range(1, n_tp):
        ag_copy(t).wait_send()


def store(*refs):
    *pairs, sem = refs
    count = len(pairs) // 2
    copies = [
        pltpu.make_async_copy(pairs[n], pairs[count + n], sem.at[n]) for n in range(count)
    ]
    for c in copies:
        c.start()
    for c in copies:
        c.wait()


def per_device(mesh_dims, *args):
    n_sp, n_tp = mesh_dims
    qm, qr, lat, rot, kw, vw, ho, og, logs = args
    heads, tok = logs.shape
    width, rdim = lat.shape[1], rot.shape[1]
    args = (qm, qr, lat, rot.T, kw, vw, ho, og, logs)
    factor = (kw.shape[1] // heads + rdim) ** (-0.5)
    span = min(SEQ_DEVICES, n_sp)
    stages = n_tp.bit_length() - 1
    rpad = -(-rdim // 128) * 128
    wide = width + rpad
    quarter = tok >> stages
    part = width // n_sp
    dma = pltpu.SemaphoreType.DMA
    scratch = [pltpu.VMEM(a.shape, a.dtype) for a in args] + [
        dma((len(args),)),
        pltpu.VMEM((span, tok, width), BF16),
        pltpu.VMEM((span, rdim, tok), BF16),
        pltpu.VMEM((heads * tok, width), BF16),
        pltpu.VMEM((heads * tok, width), BF16),
        pltpu.VMEM((heads * tok, rpad), BF16),
        pltpu.VMEM((heads * tok, width), F32),
        pltpu.VMEM((heads * tok, rdim), F32),
        pltpu.VMEM((span, tok, wide), F32),
        pltpu.VMEM((tok, wide), F32),
        pltpu.VMEM((n_sp, part, kw.shape[1]), BF16),
        pltpu.VMEM((n_sp, part, kw.shape[1]), BF16),
        pltpu.VMEM((span, quarter, wide), BF16),
        pltpu.VMEM((span, quarter, wide), BF16),
        dma((span, 2)), dma((span, 2)), dma((span, 2)), dma((span, 2)),
        dma((span,)), dma((span,)), dma((n_tp,)), dma((n_tp,)), dma((n_sp,)), dma((n_sp,)),
    ]
    halves = [pltpu.VMEM((span, tok >> (s + 1), wide), BF16) for s in range(stages)]
    sems = [dma((span,)) for s in range(stages)]
    scratch = scratch + halves + halves + sems + sems
    shapes = (
        (tok, kw.shape[1]), (tok, heads * rdim), (tok, width), (rdim, tok), (part, kw.shape[1]),
    )
    results = sum(4 * math.prod(s) for s in shapes)
    vmem = pl.BlockSpec(memory_space=pltpu.VMEM)
    hbm = pl.BlockSpec(memory_space=pltpu.HBM)
    held = pl.pallas_call(
        functools.partial(kernel, (n_sp, n_tp, heads, factor)),
        out_shape=[pltpu.VMEM(s, F32) for s in shapes],
        in_specs=[hbm] * len(args),
        out_specs=[vmem] * len(shapes),
        scratch_shapes=scratch,
        compiler_params=pltpu.CompilerParams(
            collective_id=0, has_side_effects=True, vmem_limit_bytes=VMEM_BYTES - results - (16 << 10)
        ),
        name="latent_attention_backward",
    )(*args)
    main, rotary, lat_out, rot_out, weight = pl.pallas_call(
        store,
        out_shape=[jax.ShapeDtypeStruct(s, F32) for s in shapes],
        in_specs=[vmem] * len(shapes),
        out_specs=[hbm] * len(shapes),
        scratch_shapes=[dma((len(shapes),))],
        compiler_params=pltpu.CompilerParams(vmem_limit_bytes=4 << 20),
        name="store_outputs",
    )(*held)
    return main, rotary, lat_out, rot_out.T, weight


def solution(mesh):
    dims = (mesh.shape["sp"], mesh.shape["tp"])
    return jax.shard_map(
        functools.partial(per_device, dims),
        mesh=mesh,
        in_specs=(
            P("sp", "tp"),
            P("sp", "tp"),
            P("sp", None),
            P("sp", None),
            P(None, "tp"),
            P(None, "tp"),
            P("sp", "tp"),
            P("sp", "tp"),
            P("tp", "sp"),
        ),
        out_specs=(P("sp", "tp"), P("sp", "tp"), P("sp", None), P("sp", None), P("sp", "tp")),
        check_vma=False,
    )
```

profile of v0, /device:TPU:1, one launch (start us, length us, event | category | flops | bytes accessed | tf_op | source)
XLA Modules:
  0.0 178.5 jit_solution(9566470095123586717)
XLA Ops:
  0.6 177.0 %latent_attention_backward.1 = (f32[128,512]{1,0:T(8,128)S(1)}, f32[128,256]{1,0:T(8,128)S(1)}, f32[128,512]{1,0:T(8,128)S(1)}, f32[64,128]{1,0:T(8,128)S(1)}, f32[4,512]{1,0:T(4,128)S(1)}) custom-call(bf16[128,512]{1,0:T(8,128)(2,1)} %qm_h.1, bf16[128,256]{1,0:T(8,128)(2,1)} %qr_h.1, bf16[128,512]{1,0:T(8,128)(2,1)} %lat_h.1, bf16[64,128]{1,0:T(8,128)(2,1)} %bitcast.2, ...), custom_call_target="tpu_custom_call" | custom-call | tf_op jit(solution)/shard_map/latent_attention_backward/pallas_call | solution.py:377
  177.6 0.9 store_outputs.1
where the time goes:
time: 179 us; the launch traced here: 178 us
  Pallas kernels  178 us (99%)
    pallas_call x1, Pallas kernels, per_device(): pl.pallas_call(functools.partial(kernel, (n_sp, n_tp, heads, factor)), ou...  177 us

commit v1 on v0

v1 whole, which is shorter than its diff:
```python
import functools
import math

import jax
import jax.numpy as jnp
from jax import lax
from jax.experimental import pallas as pl
from jax.experimental.pallas import tpu as pltpu
from jax.sharding import PartitionSpec as P

VMEM_BYTES = 67043328
MESH = pl.DeviceIdType.MESH
F32 = jnp.float32
BF16 = jnp.bfloat16
NX = 4
NY = 4
NZ = 16
SPAN = 4
TOK = 128
HEADS = 4
DIM = 128
RDIM = 64
WIDTH = 512
ROWS = 2 * HEADS * TOK
QUART = TOK // NY
WIDE = WIDTH + 128
PAIR = 2 * WIDTH + 128
STEPS = 2 * SPAN
SLOTS = 4
PART = 4
FACTOR = (DIM + RDIM) ** (-0.5)

DMA = pltpu.SemaphoreType.DMA


def dot(a, b, ca, cb, precision=None):
    return lax.dot_general(
        a, b, (((ca,), (cb,)), ((), ())), preferred_element_type=F32, precision=precision
    )


SCRATCH = dict(
    klat=pltpu.VMEM((SPAN, NX, TOK, WIDTH), BF16),
    krot=pltpu.VMEM((SPAN, NX, RDIM, TOK), BF16),
    qm=pltpu.VMEM((2, TOK, HEADS * DIM), BF16),
    og=pltpu.VMEM((2, TOK, HEADS * DIM), BF16),
    ho=pltpu.VMEM((2, TOK, HEADS * DIM), BF16),
    qr=pltpu.VMEM((2, TOK, HEADS * RDIM), BF16),
    lg=pltpu.VMEM((2, HEADS, TOK), F32),
    kw=pltpu.VMEM((WIDTH, HEADS * DIM), BF16),
    vw=pltpu.VMEM((WIDTH, HEADS * DIM), BF16),
    ql=pltpu.VMEM((ROWS, WIDTH), BF16),
    gr=pltpu.VMEM((ROWS, WIDTH), BF16),
    qrd=pltpu.VMEM((ROWS, 128), BF16),
    trow=pltpu.VMEM((1, ROWS), F32),
    lrow=pltpu.VMEM((1, ROWS), F32),
    mixed=pltpu.VMEM((ROWS, WIDTH), F32),
    rsum=pltpu.VMEM((ROWS, RDIM), F32),
    gf=pltpu.VMEM((SLOTS, NY, QUART, PAIR), F32),
    gst=pltpu.VMEM((STEPS, NY, QUART, PAIR), BF16),
    yin=pltpu.VMEM((STEPS, NY - 1, QUART, PAIR), BF16),
    xacc=pltpu.VMEM((SPAN, QUART, WIDE), F32),
    xst=pltpu.VMEM((SPAN, NX, QUART, WIDE), BF16),
    xin=pltpu.VMEM((SPAN, NX, QUART, WIDE), BF16),
    zst=pltpu.VMEM((SPAN, QUART, WIDE), BF16),
    zin=pltpu.VMEM((SPAN, QUART, WIDE), BF16),
    facc=pltpu.VMEM((QUART, WIDE), F32),
    obuf=pltpu.VMEM((NY, QUART, WIDE), F32),
    mrecv=pltpu.VMEM((ROWS, WIDTH // 2), F32),
    ml=pltpu.VMEM((ROWS, WIDTH // 2), BF16),
    rrecv=pltpu.VMEM((ROWS // 2, RDIM), F32),
    osend=pltpu.VMEM((TOK, HEADS * DIM), F32),
    orecv=pltpu.VMEM((TOK, HEADS * DIM), F32),
    kf=pltpu.VMEM((NX, 8, 8, HEADS * DIM), F32),
    kst=pltpu.VMEM((NX, 8, 8, HEADS * DIM), BF16),
    kxin=pltpu.VMEM((NX, 8, 8, HEADS * DIM), BF16),
    kz=pltpu.VMEM((8, 2, PART, HEADS * DIM), BF16),
    kzin=pltpu.VMEM((NZ, PART, HEADS * DIM), BF16),
    insem=DMA((9,)),
    qss=DMA((5,)), qrs=DMA((5,)),
    zks=DMA((SPAN, 2)), zkr=DMA((SPAN, 2)),
    xks=DMA((SPAN, NX, 2)), xkr=DMA((SPAN, NX, 2)),
    yss=DMA((STEPS, NY - 1)), yrs=DMA((STEPS, NY - 1)),
    xss=DMA((SPAN, NX)), xrs=DMA((SPAN, NX)),
    zss=DMA((SPAN,)), zrs=DMA((SPAN,)),
    mss=DMA((3,)), mrs=DMA((3,)),
    kxs=DMA((NX,)), kxr=DMA((NX,)),
    kzs=DMA((8, 2)), kzr=DMA((NZ,)),
    ags=DMA((NY - 1,)), agr=DMA((NY - 1,)),
)
NAMES = tuple(SCRATCH)


def rdma(src, dst, ss, rs, dev):
    return pltpu.make_async_remote_copy(
        src_ref=src, dst_ref=dst, send_sem=ss, recv_sem=rs, device_id=dev, device_id_type=MESH
    )


def kernel(qm_h, qr_h, lat_h, rot_h, kw_h, vw_h, ho_h, og_h, lg_h,
           o_main, o_rot, o_lat, o_krot, o_kw, *scratch):
    v = dict(zip(NAMES, scratch))
    klat, krot, ql, gr, qrd = v["klat"], v["krot"], v["ql"], v["gr"], v["qrd"]
    mixed, rsum, gf, gst, yin = v["mixed"], v["rsum"], v["gf"], v["gst"], v["yin"]
    trow, lrow = v["trow"], v["lrow"]
    sp = lax.axis_index("sp")
    tp = lax.axis_index("tp")
    z = sp // (2 * NX)
    x = (sp // 2) % NX
    c = sp % 2
    other = 1 - c
    xh = x // 2
    seq = (z + 1) // SPAN
    zz = z - jnp.maximum(seq * SPAN - 1, 0)
    after = jnp.minimum(seq * SPAN + SPAN - 1, NZ) - 1 - z
    partner = {"sp": sp + 1 - 2 * c}

    def at_x(xp):
        return {"sp": sp + 2 * (xp - x)}

    def at_y(yp):
        return {"tp": yp}

    barrier = pltpu.get_barrier_semaphore()

    @pl.loop(1, NZ)
    def _(d):
        zp = (z + d) % NZ
        for cp in range(2):
            pl.semaphore_signal(
                barrier, inc=1, device_id={"sp": zp * 2 * NX + 2 * x + cp}, device_id_type=MESH
            )

    pl.semaphore_signal(barrier, inc=1, device_id=partner, device_id_type=MESH)
    for d in range(1, NX):
        pl.semaphore_signal(barrier, inc=1, device_id=at_x((x + d) % NX), device_id_type=MESH)
    for d in range(1, NY):
        pl.semaphore_signal(barrier, inc=1, device_id=at_y((tp + d) % NY), device_id_type=MESH)

    shared = ("qm", "og", "ho", "qr", "lg")
    sources = (qm_h, og_h, ho_h, qr_h, lg_h)
    loads = [
        pltpu.make_async_copy(lat_h, klat.at[0, x], v["insem"].at[0]),
        pltpu.make_async_copy(rot_h, krot.at[0, x], v["insem"].at[1]),
    ]
    loads += [
        pltpu.make_async_copy(src, v[name].at[c], v["insem"].at[2 + n])
        for n, (name, src) in enumerate(zip(shared, sources))
    ]
    loads += [
        pltpu.make_async_copy(kw_h, v["kw"], v["insem"].at[7]),
        pltpu.make_async_copy(vw_h, v["vw"], v["insem"].at[8]),
    ]
    for cp in loads:
        cp.start()
    mixed[...] = jnp.zeros_like(mixed)
    rsum[...] = jnp.zeros_like(rsum)
    for cp in loads:
        cp.wait()

    def prepare(b):
        for h in range(HEADS):
            start = pl.multiple_of(b * (HEADS * TOK) + h * TOK, TOK)
            rows = pl.ds(start, TOK)
            cols = slice(h * DIM, (h + 1) * DIM)
            ql[rows] = dot(v["qm"][b, :, cols], v["kw"][:, cols], 1, 1).astype(BF16)
            og = v["og"][b, :, cols]
            gr[rows] = dot(og, v["vw"][:, cols], 1, 1).astype(BF16)
            rot = v["qr"][b, :, h * RDIM : (h + 1) * RDIM]
            qrd[rows] = jnp.concatenate([rot, rot], axis=1)
            prod = v["ho"][b, :, cols].astype(F32) * og.astype(F32)
            trow[:, rows] = dot(jnp.ones((8, DIM), F32), prod, 1, 1, lax.Precision.HIGHEST)[0:1]
            lrow[:, rows] = v["lg"][b, h : h + 1, :]

    def share(n, name):
        return rdma(v[name].at[c], v[name].at[c], v["qss"].at[n], v["qrs"].at[n], partner)

    def share_in(n, name):
        return rdma(v[name].at[other], v[name].at[other], v["qss"].at[n], v["qrs"].at[n], partner)

    keys = (klat, krot)

    def z_keys(d):
        return [
            rdma(k.at[0, x], k.at[d, x], v["zks"].at[d, n], v["zkr"].at[d, n], {"sp": sp + 2 * NX * d})
            for n, k in enumerate(keys)
        ]

    def x_keys(g, xp):
        return [
            rdma(k.at[g, x], k.at[g, x], v["xks"].at[g, xp, n], v["xkr"].at[g, x, n], at_x(xp))
            for n, k in enumerate(keys)
        ]

    def x_keys_in(g, xp):
        return [
            rdma(k.at[g, xp], k.at[g, xp], v["xks"].at[g, xp, n], v["xkr"].at[g, xp, n], at_x(xp))
            for n, k in enumerate(keys)
        ]

    prepare(c)
    pl.semaphore_wait(barrier, 2 * (NZ - 1) + 1 + NX - 1 + NY - 1)

    for n, name in enumerate(shared):
        share(n, name).start()
    for d in (1, 3, 2):
        xp = (x + d) % NX

        @pl.when(xp >= 2 * xh)
        def _():
            for cp in x_keys(0, xp):
                cp.start()

    @pl.loop(1, after + 1)
    def _(d):
        for cp in z_keys(d):
            cp.start()

    for n, name in enumerate(shared):
        share_in(n, name).wait_recv()
    prepare(other)

    def forward(g):
        @pl.when(g <= zz)
        def _():
            for cp in z_keys(g):
                cp.wait_recv()
            for d in (1, 3, 2):
                for cp in x_keys(g, (x + d) % NX):
                    cp.start()

    forward(1)

    first = 1 - xh
    last = 2 * zz + 1

    def y_copy(s, d):
        return rdma(
            gst.at[s, (tp + d) % NY], yin.at[s, d - 1], v["yss"].at[s, d - 1], v["yrs"].at[s, d - 1],
            at_y((tp + d) % NY),
        )

    def attend(s):
        g = s // 2
        m = 1 - s % 2
        for b in range(2):
            xp = 2 * m + b

            @pl.when(xp != x)
            def _():
                for cp in x_keys_in(g, xp):
                    cp.wait_recv()

        lt = klat[g, pl.ds(2 * m, 2)].reshape(2 * TOK, WIDTH)
        rt = jnp.concatenate([krot[g, 2 * m], krot[g, 2 * m + 1]], axis=1)
        scores = dot(lt, ql[...], 1, 1) + dot(rt, qrd[:, :RDIM], 0, 1)
        weights = jnp.exp(FACTOR * scores - lrow[...])
        k_id = lax.broadcasted_iota(jnp.int32, (2 * TOK, 1), 0)
        k_pos = (2 * m + k_id // TOK) * (2 * TOK) + c * TOK + k_id % TOK
        k_pos = jnp.where(g > 0, -1, k_pos)
        q_id = lax.broadcasted_iota(jnp.int32, (1, ROWS), 1)
        q_pos = (2 * x + q_id // (HEADS * TOK)) * TOK + q_id % TOK
        weights = jnp.where(k_pos <= q_pos, weights, 0.0)
        slopes = dot(lt, gr[...], 1, 1)
        dscores = weights * (slopes - trow[...])
        wl = weights.astype(BF16)
        dl = dscores.astype(BF16)
        grad = FACTOR * dot(dl, ql[...], 1, 0) + dot(wl, gr[...], 1, 0)
        slot = s % SLOTS
        gf[slot, :, :, :WIDTH] = grad[:TOK].reshape(NY, QUART, WIDTH)
        gf[slot, :, :, WIDTH : 2 * WIDTH] = grad[TOK:].reshape(NY, QUART, WIDTH)
        rgrad = FACTOR * dot(dl, qrd[...], 1, 0)
        lane = lax.broadcasted_iota(jnp.int32, (TOK, 128), 1)
        packed = jnp.where(lane < RDIM, rgrad[:TOK], rgrad[TOK:])
        gf[slot, :, :, 2 * WIDTH :] = packed.reshape(NY, QUART, 128)
        gst[s] = gf[slot].astype(BF16)
        for d in (1, 3, 2):
            y_copy(s, d).start()
        mixed[...] += dot(dl, lt, 0, 0)
        rsum[...] += dot(dl, rt, 0, 1)

    def x_copy(g, xp):
        return rdma(
            v["xst"].at[g, xp], v["xin"].at[g, x], v["xss"].at[g, xp], v["xrs"].at[g, x], at_x(xp)
        )

    def x_copy_in(g, xp):
        return rdma(
            v["xst"].at[g, xp], v["xin"].at[g, xp], v["xss"].at[g, xp], v["xrs"].at[g, xp], at_x(xp)
        )

    def reduce_y(s):
        @pl.when((s >= first) & (s <= last))
        def _():
            g = s // 2
            m = 1 - s % 2
            total = gf[s % SLOTS, tp]
            for d in range(1, NY):
                y_copy(s, d).wait_recv()
                total = total + yin[s, d - 1].astype(F32)
            for b in range(2):
                xp = 2 * m + b
                lat = total[:, b * WIDTH : (b + 1) * WIDTH]
                rot = total[:, 2 * WIDTH :]

                @pl.when(xp == x)
                def _():
                    v["xacc"][g, :, :WIDTH] = lat
                    v["xacc"][g, :, WIDTH:] = rot

                @pl.when(xp != x)
                def _():
                    v["xst"][g, xp, :, :WIDTH] = lat.astype(BF16)
                    v["xst"][g, xp, :, WIDTH:] = rot.astype(BF16)
                    x_copy(g, xp).start()

    def z_copy(g):
        return rdma(
            v["zst"].at[g], v["zin"].at[g], v["zss"].at[g], v["zrs"].at[g], {"sp": sp - 2 * NX * g}
        )

    def reduce_x(s):
        @pl.when((s >= first) & (s <= last) & (s % 2 == first))
        def _():
            g = s // 2
            v["facc"][...] = v["xacc"][g]
            for d in range(1, NX):
                xp = (x + d) % NX

                @pl.when((g > 0) | (xp >= 2 * xh))
                def _():
                    x_copy_in(g, xp).wait_recv()
                    v["facc"][...] += v["xin"][g, xp].astype(F32)

            @pl.when(g > 0)
            def _():
                v["zst"][g] = v["facc"][...].astype(BF16)
                z_copy(g).start()

            @pl.when(g == 0)
            def _():
                v["obuf"][tp] = v["facc"][...]

    @pl.loop(first, last + 1)
    def _(s):
        attend(s)

        @pl.when(s % 2 == 1)
        def _():
            forward((s + 3) // 2)

        reduce_y(s - 2)
        reduce_x(s - 3)

    half = WIDTH // 2
    mine = pl.ds(pl.multiple_of(half * c, half), half)
    theirs = pl.ds(pl.multiple_of(half * other, half), half)
    my_rows = pl.ds(pl.multiple_of(c * (ROWS // 2), ROWS // 2), ROWS // 2)
    their_rows = pl.ds(pl.multiple_of(other * (ROWS // 2), ROWS // 2), ROWS // 2)
    mix_copy = rdma(mixed.at[:, theirs], v["mrecv"], v["mss"].at[0], v["mrs"].at[0], partner)
    rot_copy = rdma(rsum.at[their_rows], v["rrecv"], v["mss"].at[1], v["mrs"].at[1], partner)
    main_copy = rdma(v["osend"], v["orecv"], v["mss"].at[2], v["mrs"].at[2], partner)
    mix_copy.start()
    rot_copy.start()
    reduce_y(last - 1)
    reduce_x(last - 2)

    mix_copy.wait_recv()
    ml = v["ml"]
    ml[...] = (mixed[:, mine] + v["mrecv"][...]).astype(BF16)

    def main_part(b, h):
        rows = pl.ds(pl.multiple_of(b * (HEADS * TOK) + h * TOK, TOK), TOK)
        return dot(ml[rows], v["kw"][mine, h * DIM : (h + 1) * DIM], 1, 0)

    for h in range(HEADS):
        v["osend"][:, h * DIM : (h + 1) * DIM] = main_part(other, h)
    main_copy.start()
    for h in range(HEADS):
        cols = slice(h * DIM, (h + 1) * DIM)
        left = jnp.concatenate(
            [ml[b * HEADS * TOK + h * TOK : b * HEADS * TOK + (h + 1) * TOK] for b in range(2)], axis=0
        )
        right = jnp.concatenate([v["qm"][b, :, cols] for b in range(2)], axis=0)
        term = (FACTOR * dot(left, right, 0, 0)).reshape(8, NX, 8, DIM)
        for xp in range(NX):
            v["kf"][xp, :, :, cols] = term[:, xp]
            v["kst"][xp, :, :, cols] = term[:, xp].astype(BF16)

    def kx_copy(xp):
        return rdma(v["kst"].at[xp], v["kxin"].at[x], v["kxs"].at[xp], v["kxr"].at[x], at_x(xp))

    def kx_copy_in(xp):
        return rdma(v["kst"].at[xp], v["kxin"].at[xp], v["kxs"].at[xp], v["kxr"].at[xp], at_x(xp))

    for d in (1, 3, 2):
        kx_copy((x + d) % NX).start()

    reduce_y(last)
    reduce_x(last - 1)
    reduce_x(last)

    total = v["kf"][x]
    for d in range(1, NX):
        xp = (x + d) % NX
        kx_copy_in(xp).wait_recv()
        total = total + v["kxin"][xp].astype(F32)
    total = total.astype(BF16)
    v["kz"][:, 0] = total[:, :PART]
    v["kz"][:, 1] = total[:, PART:]

    def kz_copy(zp, cp):
        return rdma(
            v["kz"].at[zp, cp], v["kzin"].at[z], v["kzs"].at[zp, cp], v["kzr"].at[z],
            {"sp": (8 * c + zp) * 2 * NX + 2 * x + cp},
        )

    @pl.loop(0, 8)
    def _(i):
        zp = (z + i) % 8
        for cp in range(2):
            here = (8 * c + zp == z) & (c == cp)

            @pl.when(jnp.logical_not(here))
            def _():
                kz_copy(zp, cp).start()

            @pl.when(here)
            def _():
                v["kzin"][z] = v["kz"][zp, cp]

    rot_copy.wait_recv()
    for h in range(HEADS):
        rows = pl.ds(pl.multiple_of(c * (HEADS * TOK) + h * TOK, TOK), TOK)
        o_rot[:, h * RDIM : (h + 1) * RDIM] = FACTOR * (
            rsum[rows] + v["rrecv"][h * TOK : (h + 1) * TOK]
        )
    main_copy.wait_recv()
    for h in range(HEADS):
        cols = slice(h * DIM, (h + 1) * DIM)
        o_main[:, cols] = FACTOR * (main_part(c, h) + v["orecv"][:, cols])

    @pl.loop(1, after + 1)
    def _(d):
        z_copy_in = rdma(
            v["zst"].at[d], v["zin"].at[d], v["zss"].at[d], v["zrs"].at[d], {"sp": sp + 2 * NX * d}
        )
        z_copy_in.wait_recv()
        v["obuf"][tp] += v["zin"][d].astype(F32)

    def ag_copy(d):
        return rdma(
            v["obuf"].at[tp], v["obuf"].at[tp], v["ags"].at[d - 1], v["agr"].at[d - 1],
            at_y((tp + d) % NY),
        )

    for d in (1, 3, 2):
        ag_copy(d).start()

    @pl.loop(0, NZ)
    def _(i):
        @pl.when((i != z) | (c != z // 8))
        def _():
            rdma(
                v["kz"].at[0, 0], v["kzin"].at[i], v["kzs"].at[0, 0], v["kzr"].at[i],
                {"sp": i * 2 * NX + 2 * x + z // 8},
            ).wait_recv()

    total = v["kzin"][0].astype(F32)
    for i in range(1, NZ):
        total = total + v["kzin"][i].astype(F32)
    o_kw[...] = total

    for d in range(1, NY):
        yp = (tp + NY - d) % NY
        rdma(
            v["obuf"].at[yp], v["obuf"].at[yp], v["ags"].at[d - 1], v["agr"].at[d - 1], at_y(yp)
        ).wait_recv()
    out = v["obuf"][...].reshape(TOK, WIDE)
    o_lat[...] = out[:, :WIDTH]
    flip = out[:, WIDTH:].T
    o_krot[...] = jnp.where(x % 2 == 0, flip[:RDIM], flip[RDIM:])

    for n, name in enumerate(shared):
        share(n, name).wait_send()
    for d in range(1, NX):
        xp = (x + d) % NX

        @pl.when(xp >= 2 * xh)
        def _():
            for cp in x_keys(0, xp):
                cp.wait_send()

        kx_copy(xp).wait_send()

        @pl.loop(1, zz + 1)
        def _(g):
            for cp in x_keys(g, xp):
                cp.wait_send()

        @pl.loop(0, zz + 1)
        def _(g):
            @pl.when((g > 0) | (xp // 2 <= xh))
            def _():
                x_copy(g, xp).wait_send()

    @pl.loop(1, after + 1)
    def _(d):
        for cp in z_keys(d):
            cp.wait_send()

    @pl.loop(1, zz + 1)
    def _(g):
        z_copy(g).wait_send()

    @pl.loop(first, last + 1)
    def _(s):
        for d in range(1, NY):
            y_copy(s, d).wait_send()

    mix_copy.wait_send()
    rot_copy.wait_send()
    main_copy.wait_send()

    @pl.loop(0, 8)
    def _(zp):
        for cp in range(2):
            @pl.when((8 * c + zp != z) | (c != cp))
            def _():
                kz_copy(zp, cp).wait_send()

    for d in range(1, NY):
        ag_copy(d).wait_send()


def store(*refs):
    *pairs, sem = refs
    count = len(pairs) // 2
    copies = [
        pltpu.make_async_copy(pairs[n], pairs[count + n], sem.at[n]) for n in range(count)
    ]
    for cp in copies:
        cp.start()
    for cp in copies:
        cp.wait()


def per_device(qm, qr, lat, rot, kw, vw, ho, og, logs):
    args = (qm, qr, lat, rot.T, kw, vw, ho, og, logs)
    shapes = (
        (TOK, HEADS * DIM), (TOK, HEADS * RDIM), (TOK, WIDTH), (RDIM, TOK), (PART, HEADS * DIM),
    )
    results = sum(4 * math.prod(s) for s in shapes)
    vmem = pl.BlockSpec(memory_space=pltpu.VMEM)
    hbm = pl.BlockSpec(memory_space=pltpu.HBM)
    held = pl.pallas_call(
        kernel,
        out_shape=[pltpu.VMEM(s, F32) for s in shapes],
        in_specs=[hbm] * len(args),
        out_specs=[vmem] * len(shapes),
        scratch_shapes=list(SCRATCH.values()),
        compiler_params=pltpu.CompilerParams(
            collective_id=0, has_side_effects=True, vmem_limit_bytes=VMEM_BYTES - results - (16 << 10)
        ),
        name="latent_attention_backward",
    )(*args)
    main, rotary, lat_out, rot_out, weight = pl.pallas_call(
        store,
        out_shape=[jax.ShapeDtypeStruct(s, F32) for s in shapes],
        in_specs=[vmem] * len(shapes),
        out_specs=[hbm] * len(shapes),
        scratch_shapes=[DMA((len(shapes),))],
        compiler_params=pltpu.CompilerParams(vmem_limit_bytes=4 << 20),
        name="store_outputs",
    )(*held)
    return main, rotary, lat_out, rot_out.T, weight


def solution(mesh):
    return jax.shard_map(
        per_device,
        mesh=mesh,
        in_specs=(
            P("sp", "tp"),
            P("sp", "tp"),
            P("sp", None),
            P("sp", None),
            P(None, "tp"),
            P(None, "tp"),
            P("sp", "tp"),
            P("sp", "tp"),
            P("tp", "sp"),
        ),
        out_specs=(P("sp", "tp"), P("sp", "tp"), P("sp", None), P("sp", None), P("sp", "tp")),
        check_vma=False,
    )
```

time: 179 us -> 78 us (0.44)
  Pallas kernels: 178 us -> 77 us
    pallas_call x1, Pallas kernels: 177 us -> 76.1 us  [per_device(): pl.pallas_call(kernel, out_shape=[pltpu.VMEM(s, F32) for s in shapes], in...]
where the time goes in v1:
time: 78 us; the launch traced here: 77.6 us
  Pallas kernels  77 us (99%)
    pallas_call x1, Pallas kernels, per_device(): pl.pallas_call(kernel, out_shape=[pltpu.VMEM(s, F32) for s in shapes], in...  76.1 us

profile of v1, /device:TPU:1, one launch (start us, length us, event | category | flops | bytes accessed | tf_op | source)
XLA Modules:
  0.0 77.6 jit_solution(15502139237313091009)
XLA Ops:
  0.6 76.1 %latent_attention_backward.1 = (f32[128,512]{1,0:T(8,128)S(1)}, f32[128,256]{1,0:T(8,128)S(1)}, f32[128,512]{1,0:T(8,128)S(1)}, f32[64,128]{1,0:T(8,128)S(1)}, f32[4,512]{1,0:T(4,128)S(1)}) custom-call(bf16[128,512]{1,0:T(8,128)(2,1)} %qm_h.1, bf16[128,256]{1,0:T(8,128)(2,1)} %qr_h.1, bf16[128,512]{1,0:T(8,128)(2,1)} %lat_h.1, bf16[64,128]{1,0:T(8,128)(2,1)} %bitcast.2, ...), custom_call_target="tpu_custom_call" | custom-call | tf_op jit(solution)/shard_map/latent_attention_backward/pallas_call | solution.py:556
  76.7 0.9 %store_outputs.1 = (f32[128,512]{1,0:T(8,128)}, f32[128,256]{1,0:T(8,128)}, f32[128,512]{1,0:T(8,128)}, f32[64,128]{1,0:T(8,128)}, f32[4,512]{1,0:T(4,128)}) custom-call(f32[128,512]{1,0:T(8,128)S(1)} %get-tuple-element.15.refs_0_, f32[128,256]{1,0:T(8,128)S(1)} %get-tuple-element.16.refs_1_, f32[128,512]{1,0:T(8,128)S(1)} %get-tuple-element.17.refs_2_, ...), custom_call_target="tpu_custom_call" | custom-call | tf_op jit(solution)/shard_map/store_outputs/pallas_call | solution.py:567

commit v2 on v1

--- a/solution.py
+++ b/solution.py
@@ -81,6 +81,8 @@
     zks=DMA((SPAN, 2)), zkr=DMA((SPAN, 2)),
     xks=DMA((SPAN, NX, 2)), xkr=DMA((SPAN, NX, 2)),
     yss=DMA((STEPS, NY - 1)), yrs=DMA((STEPS, NY - 1)),
+    fks=DMA((SPAN, 2, 2)), fkr=DMA((SPAN, 2, 2)),
+    far=pltpu.SemaphoreType.REGULAR((3,)),
     xss=DMA((SPAN, NX)), xrs=DMA((SPAN, NX)),
     zss=DMA((SPAN,)), zrs=DMA((SPAN,)),
     mss=DMA((3,)), mrs=DMA((3,)),
@@ -110,6 +112,9 @@
     c = sp % 2
     other = 1 - c
     xh = x // 2
+    near = x + 1 - 2 * (x % 2)
+    far = (x + 2) % NX
+    side = NX - 1 - x
     seq = (z + 1) // SPAN
     zz = z - jnp.maximum(seq * SPAN - 1, 0)
     after = jnp.minimum(seq * SPAN + SPAN - 1, NZ) - 1 - z
@@ -123,14 +128,12 @@
 
     barrier = pltpu.get_barrier_semaphore()
 
-    @pl.loop(1, NZ)
-    def _(d):
-        zp = (z + d) % NZ
+    def at_z(d, cp):
+        return {"sp": ((z + NZ + d) % NZ) * 2 * NX + 2 * x + cp}
+
+    for d in (1, -1):
         for cp in range(2):
-            pl.semaphore_signal(
-                barrier, inc=1, device_id={"sp": zp * 2 * NX + 2 * x + cp}, device_id_type=MESH
-            )
-
+            pl.semaphore_signal(barrier, inc=1, device_id=at_z(d, cp), device_id_type=MESH)
     pl.semaphore_signal(barrier, inc=1, device_id=partner, device_id_type=MESH)
     for d in range(1, NX):
         pl.semaphore_signal(barrier, inc=1, device_id=at_x((x + d) % NX), device_id_type=MESH)
@@ -199,40 +202,78 @@
         ]
 
     prepare(c)
-    pl.semaphore_wait(barrier, 2 * (NZ - 1) + 1 + NX - 1 + NY - 1)
+    pl.semaphore_wait(barrier, 4 + 1 + NX - 1 + NY - 1)
+
+    def greet(n):
+        for d in (1, -1):
+            pl.semaphore_signal(
+                v["far"].at[n], inc=1, device_id=at_z(d << n, c), device_id_type=MESH
+            )
+
+    def met(n):
+        pl.semaphore_wait(v["far"].at[n], 2)
+
+    greet(0)
 
     for n, name in enumerate(shared):
         share(n, name).start()
-    for d in (1, 3, 2):
-        xp = (x + d) % NX
-
+
+    def send_up(d):
+        @pl.when(d <= after)
+        def _():
+            for cp in z_keys(d):
+                cp.start()
+
+    send_up(1)
+    for xp in (near, side, far):
         @pl.when(xp >= 2 * xh)
         def _():
             for cp in x_keys(0, xp):
                 cp.start()
-
-    @pl.loop(1, after + 1)
-    def _(d):
-        for cp in z_keys(d):
-            cp.start()
 
     for n, name in enumerate(shared):
         share_in(n, name).wait_recv()
     prepare(other)
+    met(0)
+    send_up(2)
+    greet(1)
 
     def forward(g):
         @pl.when(g <= zz)
         def _():
             for cp in z_keys(g):
                 cp.wait_recv()
-            for d in (1, 3, 2):
-                for cp in x_keys(g, (x + d) % NX):
+            for xp in (near, side):
+                for cp in x_keys(g, xp):
                     cp.start()
 
     forward(1)
-
-    first = 1 - xh
     last = 2 * zz + 1
+
+    def pass_on(g, i):
+        src, dst = ((near, side), (side, near))[i]
+        out = []
+        for n, (k, size) in enumerate(((klat, TOK // 2), (krot, RDIM // 2))):
+            part = k.at[g, src, pl.ds(i * size, size)]
+            out.append(
+                rdma(part, part, v["fks"].at[g, i, n], v["fkr"].at[g, i, n], at_x(dst))
+            )
+        return out
+
+    def passed_in(g, i):
+        out = []
+        for n, (k, size) in enumerate(((klat, TOK // 2), (krot, RDIM // 2))):
+            part = k.at[g, far, pl.ds(i * size, size)]
+            out.append(
+                rdma(part, part, v["fks"].at[g, i, n], v["fkr"].at[g, i, n], at_x((near, side)[1 - i]))
+            )
+        return out
+
+    def pair_of(s):
+        return xh + (s % 2) * (1 - 2 * xh)
+
+    def valid(s):
+        return (s >= 0) & (s <= last) & ((s != 1) | (xh == 1))
 
     def y_copy(s, d):
         return rdma(
@@ -242,13 +283,31 @@
 
     def attend(s):
         g = s // 2
-        m = 1 - s % 2
-        for b in range(2):
-            xp = 2 * m + b
-
-            @pl.when(xp != x)
+        m = pair_of(s)
+
+        @pl.when(s % 2 == 0)
+        def _():
+            for cp in x_keys_in(g, near):
+                cp.wait_recv()
+
+            @pl.when(g > 0)
             def _():
-                for cp in x_keys_in(g, xp):
+                for cp in x_keys_in(g, side):
+                    cp.wait_recv()
+                for i in range(2):
+                    for cp in pass_on(g, i):
+                        cp.start()
+
+        @pl.when((s % 2 == 1) & (g > 0))
+        def _():
+            for i in range(2):
+                for cp in passed_in(g, i):
+                    cp.wait_recv()
+
+        @pl.when(s == 1)
+        def _():
+            for xp in (side, far):
+                for cp in x_keys_in(0, xp):
                     cp.wait_recv()
 
         lt = klat[g, pl.ds(2 * m, 2)].reshape(2 * TOK, WIDTH)
@@ -290,10 +349,10 @@
         )
 
     def reduce_y(s):
-        @pl.when((s >= first) & (s <= last))
+        @pl.when(valid(s))
         def _():
             g = s // 2
-            m = 1 - s % 2
+            m = pair_of(s)
             total = gf[s % SLOTS, tp]
             for d in range(1, NY):
                 y_copy(s, d).wait_recv()
@@ -320,7 +379,7 @@
         )
 
     def reduce_x(s):
-        @pl.when((s >= first) & (s <= last) & (s % 2 == first))
+        @pl.when((s >= 0) & (s <= last) & (s % 2 == 1))
         def _():
             g = s // 2
             v["facc"][...] = v["xacc"][g]
@@ -341,13 +400,21 @@
             def _():
                 v["obuf"][tp] = v["facc"][...]
 
-    @pl.loop(first, last + 1)
+    @pl.loop(0, last + 1)
     def _(s):
-        attend(s)
-
-        @pl.when(s % 2 == 1)
-        def _():
-            forward((s + 3) // 2)
+        @pl.when(valid(s))
+        def _():
+            attend(s)
+
+        @pl.when((s % 2 == 0) & (s > 0))
+        def _():
+            forward(s // 2 + 1)
+
+        @pl.when(s == 0)
+        def _():
+            met(1)
+            send_up(3)
+            greet(2)
 
         reduce_y(s - 2)
         reduce_x(s - 3)
@@ -397,8 +464,6 @@
         kx_copy((x + d) % NX).start()
 
     reduce_y(last)
-    reduce_x(last - 1)
-    reduce_x(last)
 
     total = v["kf"][x]
     for d in range(1, NX):
@@ -415,6 +480,8 @@
             {"sp": (8 * c + zp) * 2 * NX + 2 * x + cp},
         )
 
+    met(2)
+
     @pl.loop(0, 8)
     def _(i):
         zp = (z + i) % 8
@@ -429,6 +496,7 @@
             def _():
                 v["kzin"][z] = v["kz"][zp, cp]
 
+    reduce_x(last)
     rot_copy.wait_recv()
     for h in range(HEADS):
         rows = pl.ds(pl.multiple_of(c * (HEADS * TOK) + h * TOK, TOK), TOK)
@@ -483,20 +551,22 @@
 
     for n, name in enumerate(shared):
         share(n, name).wait_send()
-    for d in range(1, NX):
-        xp = (x + d) % NX
-
+    @pl.loop(1, zz + 1)
+    def _(g):
+        for xp in (near, side):
+            for cp in x_keys(g, xp):
+                cp.wait_send()
+        for i in range(2):
+            for cp in pass_on(g, i):
+                cp.wait_send()
+
+    for xp in (near, side, far):
         @pl.when(xp >= 2 * xh)
         def _():
             for cp in x_keys(0, xp):
                 cp.wait_send()
 
         kx_copy(xp).wait_send()
-
-        @pl.loop(1, zz + 1)
-        def _(g):
-            for cp in x_keys(g, xp):
-                cp.wait_send()
 
         @pl.loop(0, zz + 1)
         def _(g):
@@ -513,10 +583,12 @@
     def _(g):
         z_copy(g).wait_send()
 
-    @pl.loop(first, last + 1)
+    @pl.loop(0, last + 1)
     def _(s):
-        for d in range(1, NY):
-            y_copy(s, d).wait_send()
+        @pl.when(valid(s))
+        def _():
+            for d in range(1, NY):
+                y_copy(s, d).wait_send()
 
     mix_copy.wait_send()
     rot_copy.wait_send()

time: 78 us -> 69.4 us (0.89)
  Pallas kernels: 77 us -> 68.6 us
    pallas_call x1, Pallas kernels: 76.1 us -> 67.7 us  [per_device(): pl.pallas_call(kernel, out_shape=[pltpu.VMEM(s, F32) for s in shapes], in...]
where the time goes in v2:
time: 69.4 us; the launch traced here: 69.3 us
  Pallas kernels  68.6 us (99%)
    pallas_call x1, Pallas kernels, per_device(): pl.pallas_call(kernel, out_shape=[pltpu.VMEM(s, F32) for s in shapes], in...  67.7 us

profile of v2, /device:TPU:1, one launch (start us, length us, event | category | flops | bytes accessed | tf_op | source)
XLA Modules:
  0.0 69.3 jit_solution(7391861032331918756)
XLA Ops:
  0.6 67.7 %latent_attention_backward.1 = (f32[128,512]{1,0:T(8,128)S(1)}, f32[128,256]{1,0:T(8,128)S(1)}, f32[128,512]{1,0:T(8,128)S(1)}, f32[64,128]{1,0:T(8,128)S(1)}, f32[4,512]{1,0:T(4,128)S(1)}) custom-call(bf16[128,512]{1,0:T(8,128)(2,1)} %qm_h.1, bf16[128,256]{1,0:T(8,128)(2,1)} %qr_h.1, bf16[128,512]{1,0:T(8,128)(2,1)} %lat_h.1, bf16[64,128]{1,0:T(8,128)(2,1)} %bitcast.2, ...), custom_call_target="tpu_custom_call" | custom-call | tf_op jit(solution)/shard_map/latent_attention_backward/pallas_call | solution.py:628
  68.4 0.9 %store_outputs.1 = (f32[128,512]{1,0:T(8,128)}, f32[128,256]{1,0:T(8,128)}, f32[128,512]{1,0:T(8,128)}, f32[64,128]{1,0:T(8,128)}, f32[4,512]{1,0:T(4,128)}) custom-call(f32[128,512]{1,0:T(8,128)S(1)} %get-tuple-element.15.refs_0_, f32[128,256]{1,0:T(8,128)S(1)} %get-tuple-element.16.refs_1_, f32[128,512]{1,0:T(8,128)S(1)} %get-tuple-element.17.refs_2_, ...), custom_call_target="tpu_custom_call" | custom-call | tf_op jit(solution)/shard_map/store_outputs/pallas_call | solution.py:639

commit v3 on v2

--- a/solution.py
+++ b/solution.py
@@ -183,12 +183,6 @@
 
     keys = (klat, krot)
 
-    def z_keys(d):
-        return [
-            rdma(k.at[0, x], k.at[d, x], v["zks"].at[d, n], v["zkr"].at[d, n], {"sp": sp + 2 * NX * d})
-            for n, k in enumerate(keys)
-        ]
-
     def x_keys(g, xp):
         return [
             rdma(k.at[g, x], k.at[g, x], v["xks"].at[g, xp, n], v["xkr"].at[g, x, n], at_x(xp))
@@ -218,10 +212,19 @@
     for n, name in enumerate(shared):
         share(n, name).start()
 
+    def lift(d):
+        return [
+            rdma(
+                k.at[d - 1, x], k.at[d, x], v["zks"].at[d, n], v["zkr"].at[d, n],
+                {"sp": sp + 2 * NX},
+            )
+            for n, k in enumerate(keys)
+        ]
+
     def send_up(d):
-        @pl.when(d <= after)
-        def _():
-            for cp in z_keys(d):
+        @pl.when((after > 0) & (d < SPAN))
+        def _():
+            for cp in lift(d):
                 cp.start()
 
     send_up(1)
@@ -235,19 +238,18 @@
         share_in(n, name).wait_recv()
     prepare(other)
     met(0)
-    send_up(2)
     greet(1)
 
     def forward(g):
         @pl.when(g <= zz)
         def _():
-            for cp in z_keys(g):
+            for cp in lift(g):
                 cp.wait_recv()
+            send_up(g + 1)
             for xp in (near, side):
                 for cp in x_keys(g, xp):
                     cp.start()
 
-    forward(1)
     last = 2 * zz + 1
 
     def pass_on(g, i):
@@ -297,6 +299,7 @@
                 for i in range(2):
                     for cp in pass_on(g, i):
                         cp.start()
+                forward(g + 1)
 
         @pl.when((s % 2 == 1) & (g > 0))
         def _():
@@ -406,14 +409,13 @@
         def _():
             attend(s)
 
-        @pl.when((s % 2 == 0) & (s > 0))
-        def _():
-            forward(s // 2 + 1)
-
         @pl.when(s == 0)
         def _():
+            forward(1)
+
+        @pl.when(s == 0)
+        def _():
             met(1)
-            send_up(3)
             greet(2)
 
         reduce_y(s - 2)
@@ -429,9 +431,6 @@
     main_copy = rdma(v["osend"], v["orecv"], v["mss"].at[2], v["mrs"].at[2], partner)
     mix_copy.start()
     rot_copy.start()
-    reduce_y(last - 1)
-    reduce_x(last - 2)
-
     mix_copy.wait_recv()
     ml = v["ml"]
     ml[...] = (mixed[:, mine] + v["mrecv"][...]).astype(BF16)
@@ -440,9 +439,6 @@
         rows = pl.ds(pl.multiple_of(b * (HEADS * TOK) + h * TOK, TOK), TOK)
         return dot(ml[rows], v["kw"][mine, h * DIM : (h + 1) * DIM], 1, 0)
 
-    for h in range(HEADS):
-        v["osend"][:, h * DIM : (h + 1) * DIM] = main_part(other, h)
-    main_copy.start()
     for h in range(HEADS):
         cols = slice(h * DIM, (h + 1) * DIM)
         left = jnp.concatenate(
@@ -463,6 +459,11 @@
     for d in (1, 3, 2):
         kx_copy((x + d) % NX).start()
 
+    for h in range(HEADS):
+        v["osend"][:, h * DIM : (h + 1) * DIM] = main_part(other, h)
+    main_copy.start()
+    reduce_y(last - 1)
+    reduce_x(last - 2)
     reduce_y(last)
 
     total = v["kf"][x]
@@ -574,10 +575,12 @@
             def _():
                 x_copy(g, xp).wait_send()
 
-    @pl.loop(1, after + 1)
-    def _(d):
-        for cp in z_keys(d):
-            cp.wait_send()
+    @pl.when(after > 0)
+    def _():
+        @pl.loop(1, zz + 2)
+        def _(d):
+            for cp in lift(d):
+                cp.wait_send()
 
     @pl.loop(1, zz + 1)
     def _(g):

time: 69.4 us -> 64.2 us (0.925)
  the two profiles are of different devices: /device:TPU:1 before, /device:TPU:96 now
where the time goes in v3:
time: 64.2 us; the launch traced here: 64 us
  Pallas kernels  63.4 us (99%)
    pallas_call x1, Pallas kernels, per_device(): pl.pallas_call(kernel, out_shape=[pltpu.VMEM(s, F32) for s in shapes], in...  62.5 us

profile of v3, /device:TPU:96, one launch (start us, length us, event | category | flops | bytes accessed | tf_op | source)
XLA Modules:
  0.0 64.0 jit_solution(17438192838375235692)
XLA Ops:
  0.6 62.5 %latent_attention_backward.1 = (f32[128,512]{1,0:T(8,128)S(1)}, f32[128,256]{1,0:T(8,128)S(1)}, f32[128,512]{1,0:T(8,128)S(1)}, f32[64,128]{1,0:T(8,128)S(1)}, f32[4,512]{1,0:T(4,128)S(1)}) custom-call(bf16[128,512]{1,0:T(8,128)(2,1)} %qm_h.1, bf16[128,256]{1,0:T(8,128)(2,1)} %qr_h.1, bf16[128,512]{1,0:T(8,128)(2,1)} %lat_h.1, bf16[64,128]{1,0:T(8,128)(2,1)} %bitcast.2, ...), custom_call_target="tpu_custom_call" | custom-call | tf_op jit(solution)/shard_map/latent_attention_backward/pallas_call | solution.py:631
  63.1 0.9 %store_outputs.1 = (f32[128,512]{1,0:T(8,128)}, f32[128,256]{1,0:T(8,128)}, f32[128,512]{1,0:T(8,128)}, f32[64,128]{1,0:T(8,128)}, f32[4,512]{1,0:T(4,128)}) custom-call(f32[128,512]{1,0:T(8,128)S(1)} %get-tuple-element.15.refs_0_, f32[128,256]{1,0:T(8,128)S(1)} %get-tuple-element.16.refs_1_, f32[128,512]{1,0:T(8,128)S(1)} %get-tuple-element.17.refs_2_, ...), custom_call_target="tpu_custom_call" | custom-call | tf_op jit(solution)/shard_map/store_outputs/pallas_call | solution.py:642

commit v4 on v3

--- a/solution.py
+++ b/solution.py
@@ -336,7 +336,7 @@
         packed = jnp.where(lane < RDIM, rgrad[:TOK], rgrad[TOK:])
         gf[slot, :, :, 2 * WIDTH :] = packed.reshape(NY, QUART, 128)
         gst[s] = gf[slot].astype(BF16)
-        for d in (1, 3, 2):
+        for d in (2, 1, 3):
             y_copy(s, d).start()
         mixed[...] += dot(dl, lt, 0, 0)
         rsum[...] += dot(dl, rt, 0, 1)
@@ -456,7 +456,7 @@
     def kx_copy_in(xp):
         return rdma(v["kst"].at[xp], v["kxin"].at[xp], v["kxs"].at[xp], v["kxr"].at[xp], at_x(xp))
 
-    for d in (1, 3, 2):
+    for d in (2, 1, 3):
         kx_copy((x + d) % NX).start()
 
     for h in range(HEADS):
@@ -523,7 +523,7 @@
             at_y((tp + d) % NY),
         )
 
-    for d in (1, 3, 2):
+    for d in (2, 1, 3):
         ag_copy(d).start()
 
     @pl.loop(0, NZ)

time: 64.2 us -> 63.7 us (level)
  the two profiles are of different devices: /device:TPU:96 before, /device:TPU:99 now
where the time goes in v4:
time: 63.7 us; the launch traced here: 63.6 us
  Pallas kernels  62.9 us (99%)
  between operations  0.64 us (1%)
    pallas_call x1, Pallas kernels, per_device(): pl.pallas_call(kernel, out_shape=[pltpu.VMEM(s, F32) for s in shapes], in...  62 us

profile of v4, /device:TPU:99, one launch (start us, length us, event | category | flops | bytes accessed | tf_op | source)
XLA Modules:
  0.0 63.6 jit_solution(14560743324875124441)
XLA Ops:
  0.6 62.0 %latent_attention_backward.1 = (f32[128,512]{1,0:T(8,128)S(1)}, f32[128,256]{1,0:T(8,128)S(1)}, f32[128,512]{1,0:T(8,128)S(1)}, f32[64,128]{1,0:T(8,128)S(1)}, f32[4,512]{1,0:T(4,128)S(1)}) custom-call(bf16[128,512]{1,0:T(8,128)(2,1)} %qm_h.1, bf16[128,256]{1,0:T(8,128)(2,1)} %qr_h.1, bf16[128,512]{1,0:T(8,128)(2,1)} %lat_h.1, bf16[64,128]{1,0:T(8,128)(2,1)} %bitcast.2, ...), custom_call_target="tpu_custom_call" | custom-call | tf_op jit(solution)/shard_map/latent_attention_backward/pallas_call | solution.py:631
  62.7 0.9 %store_outputs.1 = (f32[128,512]{1,0:T(8,128)}, f32[128,256]{1,0:T(8,128)}, f32[128,512]{1,0:T(8,128)}, f32[64,128]{1,0:T(8,128)}, f32[4,512]{1,0:T(4,128)}) custom-call(f32[128,512]{1,0:T(8,128)S(1)} %get-tuple-element.15.refs_0_, f32[128,256]{1,0:T(8,128)S(1)} %get-tuple-element.16.refs_1_, f32[128,512]{1,0:T(8,128)S(1)} %get-tuple-element.17.refs_2_, ...), custom_call_target="tpu_custom_call" | custom-call | tf_op jit(solution)/shard_map/store_outputs/pallas_call | solution.py:642
